TPU v7x, 32 devices: a whole 2x2x4 slice. The times are simulated.
32 devices in a mesh: fs: 8 (over z, y), tp: 4 (over x, core).
Axes of the slice: x: 2, y: 2, z: 4, core: 2. Of those that a mesh axis runs over, the one named last changes fastest.
Arguments:
- inputs: bfloat16 [16384, 2048], P('fs'), may hold values from -6 to 6
- attn_out: bfloat16 [16384, 1024], P('fs', 'tp'), may hold values from -6 to 6
- grad_query: bfloat16 [16384, 1024], P('fs', 'tp'), may hold values from -0.125 to 0.125
- grad_key: bfloat16 [16384, 1024], P('fs', 'tp'), may hold values from -0.125 to 0.125
- grad_mixed: bfloat16 [16384, 2048], P('fs'), may hold values from -0.15625 to 0.15625
- query_weight: float32 [2048, 1024], P('fs', 'tp'), may hold values from -0.75 to 0.75
- key_weight: float32 [2048, 1024], P('fs', 'tp'), may hold values from -0.75 to 0.75
- out_weight: float32 [1024, 2048], P('tp', 'fs'), may hold values from -0.75 to 0.75
- factors: bfloat16 [3, 2048, 256], P(None, 'fs'), may hold values from -0.125 to 0.125
- moment_first: float32 [3, 256, 1024], P(None, 'fs', 'tp'), may hold values from -6 to 6
- moment_second: float32 [3, 256, 1024], P(None, 'fs', 'tp'), may hold values from 0.05 to 2
Outputs:
- step_query: float32 [2048, 1024], P('fs', 'tp')
- step_key: float32 [2048, 1024], P('fs', 'tp')
- step_out: float32 [1024, 2048], P('tp', 'fs')
- copy_query: bfloat16 [2048, 1024], P(None, 'tp')
- copy_key: bfloat16 [2048, 1024], P(None, 'tp')
- copy_out: bfloat16 [1024, 2048], P('tp')
- first_new: float32 [3, 256, 1024], P(None, 'fs', 'tp')
- second_new: float32 [3, 256, 1024], P(None, 'fs', 'tp')
All inputs are finite; a program needn't handle non-finite values.
Results may differ from a plain program's by a relative error of at most 0.006.
Values may be sent and summed in bfloat16 or wider, within the bound.
A program may use at most 128 MiB of HBM per device.

v0:
```python
import jax
import jax.numpy as jnp
from jax import lax
from jax.sharding import PartitionSpec as P

RANK = 256
HW = 1024
first_decay = 0.8
second_decay = 0.9
epsilon = 1e-08
learn_rate = 0.02


def over_tokens(left_side, right_side):
    return jnp.dot(left_side.T, right_side, preferred_element_type=jnp.float32)


def moments_update(projected, old_first, old_second):
    first_new = first_decay * old_first + (1.0 - first_decay) * projected
    second_new = second_decay * old_second + (1.0 - second_decay) * projected * projected
    adam_ratio = first_new / (jnp.sqrt(second_new) + epsilon)
    return (first_new, second_new, adam_ratio)


def per_device(
    inputs,
    attn_out,
    grad_query,
    grad_key,
    grad_mixed,
    query_weight,
    key_weight,
    out_weight,
    factors,
    moment_first,
    moment_second,
):
    pairs = ((inputs, grad_query), (inputs, grad_key), (grad_mixed, attn_out))
    partial_value = []
    whole_factors = lax.all_gather(factors, "fs", axis=1, tiled=True)
    for matrix_number in range(3):
        left_side, right_side = pairs[matrix_number]
        mapped = jnp.dot(
            left_side, whole_factors[matrix_number], preferred_element_type=jnp.float32
        )
        upper_part = mapped.astype(jnp.bfloat16)
        lower_part = (mapped - upper_part.astype(jnp.float32)).astype(jnp.bfloat16)
        partial_value.append(
            over_tokens(upper_part, right_side) + over_tokens(lower_part, right_side)
        )
    partial_sums = jnp.stack(partial_value)
    reduced = lax.psum_scatter(partial_sums, "fs", scatter_dimension=1, tiled=True)
    first_new, second_new, adam_ratio = moments_update(reduced, moment_first, moment_second)
    square_total = lax.psum(jnp.sum(adam_ratio * adam_ratio), ("fs", "tp"))
    directions = lax.all_gather(adam_ratio.astype(jnp.bfloat16), "fs", axis=1, tiled=True)
    step_scale = lax.rsqrt(square_total / (3 * RANK * HW) + 1.0)
    step_query = step_scale * jnp.dot(factors[0], directions[0], preferred_element_type=jnp.float32)
    step_key = step_scale * jnp.dot(factors[1], directions[1], preferred_element_type=jnp.float32)
    step_out = step_scale * jnp.dot(factors[2], directions[2], preferred_element_type=jnp.float32).T
    new_query = (query_weight - learn_rate * step_query).astype(jnp.bfloat16)
    new_key = (key_weight - learn_rate * step_key).astype(jnp.bfloat16)
    new_out = (out_weight - learn_rate * step_out).astype(jnp.bfloat16)
    copy_query, copy_key, copy_out = (
        lax.all_gather(new_query, "fs", axis=0, tiled=True),
        lax.all_gather(new_key, "fs", axis=0, tiled=True),
        lax.all_gather(new_out, "fs", axis=1, tiled=True),
    )
    return (step_query, step_key, step_out, copy_query, copy_key, copy_out, first_new, second_new)


def solution(mesh):
    in_specs = (
        P("fs", None),
        P("fs", "tp"),
        P("fs", "tp"),
        P("fs", "tp"),
        P("fs", None),
        P("fs", "tp"),
        P("fs", "tp"),
        P("tp", "fs"),
        P(None, "fs", None),
        P(None, "fs", "tp"),
        P(None, "fs", "tp"),
    )
    out_specs = (
        P("fs", "tp"),
        P("fs", "tp"),
        P("tp", "fs"),
        P(None, "tp"),
        P(None, "tp"),
        P("tp", None),
        P(None, "fs", "tp"),
        P(None, "fs", "tp"),
    )
    return jax.shard_map(
        per_device, mesh=mesh, in_specs=in_specs, out_specs=out_specs, check_vma=False
    )
```

profile of v0, /device:TPU:0, one launch (start us, length us, event | category | flops | bytes accessed | tf_op | source)
XLA Modules:
  0.0 357.2 jit_solution(18089917660759252237)
XLA Ops:
  7.2 0.0 copy-start
  7.2 0.0 all-gather.5.cloned.1.call-start
  7.2 0.7 all-gather.5.cloned.1.call-update
  7.9 0.0 reduce-scatter.2.cloned.1.call-start
  8.0 65.0 %all-gather.5.cloned.1.call-done = bf16[3,2048,256]{2,1,0:T(8,128)(2,1)} async-done(((bf16[3,256,256]{2,1,0:T(8,128)(2,1)}), bf16[3,2048,256]{2,1,0:T(8,128)(2,1)}) %all-gather.5.cloned.1.call-update) | async-done | bytes 3145744 | tf_op jit(solution)/shard_map/all_gather | solution.py:40
  73.0 0.0 copy-start.12
  73.0 6.2 %fusion.6 = f32[2048,256]{1,0:T(8,128)S(1)} fusion(bf16[2048,2048]{1,0:T(8,128)(2,1)} %param.11, bf16[3,2048,256]{2,1,0:T(8,128)(2,1)} %all-gather.5.cloned.1.call-done), kind=kOutput, calls=%fused_computation.17 | convolution fusion | flops 2147483648 | bytes 11534336 | tf_op jit(solution)/shard_map/dot_general | solution.py:43
  79.2 0.0 copy-done
  79.2 0.0 copy-start.13
  79.2 0.5 fusion.12
  79.7 0.0 slice-start
  79.7 0.5 fusion.3
  80.2 0.0 copy-done.12
  80.2 0.9 copy-done.13
  81.1 2.4 fusion.7
  83.6 0.0 copy-done.1
  83.6 0.5 fusion.15
  84.0 0.5 fusion.4
  84.5 0.0 slice-done
  84.5 0.0 slice-done.1
  84.6 0.0 copy-start.2
  84.6 2.4 fusion.5
  87.0 0.0 copy-done.2
  87.0 0.5 fusion.9
  87.5 0.5 fusion.2
  88.0 0.0 copy-start.8
  88.0 0.0 copy-start.10
  88.0 0.0 copy-start.11
  88.0 0.0 copy-start.3
  88.1 0.9 pad_maximum_fusion
  89.0 0.0 reduce-scatter.2.cloned.1.call-update
  89.0 0.0 copy-start.9
  89.0 0.0 all-gather.11.cloned.1.call-start
  89.1 0.0 copy-done.8
  89.1 0.1 copy.24
  89.2 62.6 %reduce-scatter.2.cloned.1.call-done = f32[3,32,256]{2,1,0:T(8,128)} async-done(((f32[3,256,256]{2,1,0:T(8,128)}), f32[3,32,256]{2,1,0:T(8,128)}) %reduce-scatter.2.cloned.1.call-update) | async-done | bytes 98320 | tf_op jit(solution)/shard_map/reduce_scatter | solution.py:52
  151.8 0.0 copy-done.10
  151.8 0.0 copy-done.11
  151.8 1.6 multiply_reduce_fusion
  153.4 31.2 %all_gather.16 = bf16[3,256,256]{2,1,0:T(8,128)(2,1)S(1)} all-gather(bf16[3,32,256]{2,1,0:T(8,128)(2,1)S(1)} %fusion.24), channel_id=1, replica_groups=mesh['fs'=8,'tp'=4] {'fs'}, dimensions={1}, use_global_device_ids=true | all-gather | bytes 442368 | tf_op jit(solution)/shard_map/all_gather | solution.py:55
  184.6 37.6 %psum.7 = f32[]{:T(128)} all-reduce(f32[]{:T(128)} %get-tuple-element.16), channel_id=1, replica_groups=mesh['fs'=8,'tp'=4] {'fs','tp'}, use_global_device_ids=true, to_apply=%region_2.0 | all-reduce | flops 1 | bytes 8 | tf_op jit(solution)/shard_map/psum | solution.py:54
  222.9 0.0 copy-done.3
  222.9 0.8 subtract_convert_fusion.6
  223.8 0.0 all-gather.11.cloned.1.call-update
  223.8 0.0 all-gather.9.cloned.1.call-start
  223.8 0.0 copy-done.7
  223.8 0.9 subtract_convert_fusion.7
  224.8 0.0 all-gather.9.cloned.1.call-update
  224.8 0.0 all-gather.7.cloned.1.call-start
  224.9 0.0 copy-done.9
  224.9 0.1 copy.22
  225.0 0.9 subtract_convert_fusion.8
  225.9 0.0 copy-done.5
  225.9 0.0 copy-done.6
  225.9 0.0 all-gather.7.cloned.1.call-update
  225.9 0.8 copy.26
  226.8 0.8 copy.25
  227.6 37.6 %all-gather.11.cloned.1.call-done = bf16[256,2048]{0,1:T(8,128)(2,1)} async-done(((bf16[256,256]{0,1:T(8,128)(2,1)}), bf16[256,2048]{0,1:T(8,128)(2,1)}) %all-gather.11.cloned.1.call-update) | async-done | bytes 1048592 | tf_op jit(solution)/shard_map/all_gather | solution.py:66
  265.2 2.3 copy.28
  267.5 39.3 %all-gather.9.cloned.1.call-done = bf16[2048,256]{1,0:T(8,128)(2,1)} async-done(((bf16[256,256]{1,0:T(8,128)(2,1)}), bf16[2048,256]{1,0:T(8,128)(2,1)}) %all-gather.9.cloned.1.call-update) | async-done | bytes 1048592 | tf_op jit(solution)/shard_map/all_gather | solution.py:65
  306.8 40.6 %all-gather.7.cloned.1.call-done = bf16[2048,256]{0,1:T(8,128)(2,1)} async-done(((bf16[256,256]{0,1:T(8,128)(2,1)}), bf16[2048,256]{0,1:T(8,128)(2,1)}) %all-gather.7.cloned.1.call-update) | async-done | bytes 1048592 | tf_op jit(solution)/shard_map/all_gather | solution.py:64
  347.4 2.3 copy.27
  349.7 0.0 copy-done.4
  349.7 1.0 copy.32
  (8 shorter events, 0.1 us)
Async XLA Ops:
  7.2 72.0 %copy-start = (bf16[2048,256]{1,0:T(8,128)(2,1)S(1)}, bf16[2048,256]{1,0:T(8,128)(2,1)}, u32[]{:S(2)}) copy-start(bf16[2048,256]{1,0:T(8,128)(2,1)} %param.14) | copy-start | bytes 3145732
  7.2 65.8 %all-gather.5.cloned.1.call-start = ((), (), s32[]{:S(2)}) async-start(), calls=%async_computation.1 | async-start | bytes 3538944 | tf_op jit(solution)/shard_map/all_gather | solution.py:40
  7.9 143.9 %reduce-scatter.2.cloned.1.call-start = ((), (), s32[]{:S(2)}) async-start(), calls=%async_computation.2 | async-start | bytes 884736 | tf_op jit(solution)/shard_map/reduce_scatter | solution.py:52
  73.0 7.3 %copy-start.12 = (bf16[2048,2048]{1,0:T(8,128)(2,1)S(1)}, bf16[2048,2048]{1,0:T(8,128)(2,1)}, u32[]{:S(2)}) copy-start(bf16[2048,2048]{1,0:T(8,128)(2,1)} %param.11) | copy-start | bytes 25165828
  79.2 1.9 copy-start.13
  79.7 4.8 %slice-start = ((s8[8388608]{0:T(1024)(128)(4,1)}), s8[4194304]{0:T(1024)(128)(4,1)S(1)}, s32[]{:S(2)}) async-start(s8[8388608]{0:T(1024)(128)(4,1)} %bitcast.58), calls=%async_computation.6 | async-start | bytes 8388608
  81.1 2.5 copy-start.1
  81.1 3.4 slice-start.1
  84.6 2.5 copy-start.2
  88.0 1.1 copy-start.8
  88.0 63.8 %copy-start.10 = (f32[3,32,256]{2,1,0:T(8,128)S(1)}, f32[3,32,256]{2,1,0:T(8,128)}, u32[]{:S(2)}) copy-start(f32[3,32,256]{2,1,0:T(8,128)} %param.21) | copy-start | bytes 294916
  88.0 63.8 %copy-start.11 = (f32[3,32,256]{2,1,0:T(8,128)S(1)}, f32[3,32,256]{2,1,0:T(8,128)}, u32[]{:S(2)}) copy-start(f32[3,32,256]{2,1,0:T(8,128)} %param.20) | copy-start | bytes 294916
  88.0 134.9 %copy-start.3 = (bf16[3,256,256]{2,1,0:T(8,128)(2,1)S(1)}, bf16[3,256,256]{2,1,0:T(8,128)(2,1)}, u32[]{:S(2)}) copy-start(bf16[3,256,256]{2,1,0:T(8,128)(2,1)} %param.19) | copy-start | bytes 1179652
  89.0 134.9 %copy-start.7 = (f32[256,256]{1,0:T(8,128)S(1)}, f32[256,256]{1,0:T(8,128)}, u32[]{:S(2)}) copy-start(f32[256,256]{1,0:T(8,128)} %param.17) | copy-start | bytes 786436
  89.0 135.8 %copy-start.9 = (f32[256,256]{1,0:T(8,128)S(1)}, f32[256,256]{1,0:T(8,128)}, u32[]{:S(2)}) copy-start(f32[256,256]{1,0:T(8,128)} %param.16) | copy-start | bytes 786436
  89.0 176.2 %all-gather.11.cloned.1.call-start = ((), (), s32[]{:S(2)}) async-start(), calls=%async_computation.5 | async-start | bytes 1179648 | tf_op jit(solution)/shard_map/all_gather | solution.py:66
  153.4 72.5 %copy-start.5 = (f32[3,32,256]{2,1,0:T(8,128)}, f32[3,32,256]{2,1,0:T(8,128)S(1)}, u32[]{:S(2)}) copy-start(f32[3,32,256]{2,1,0:T(8,128)S(1)} %get-tuple-element.40) | copy-start | bytes 294916
  153.4 72.5 %copy-start.6 = (f32[3,32,256]{2,1,0:T(8,128)}, f32[3,32,256]{2,1,0:T(8,128)S(1)}, u32[]{:S(2)}) copy-start(f32[3,32,256]{2,1,0:T(8,128)S(1)} %get-tuple-element.39) | copy-start | bytes 294916
  223.8 83.0 %all-gather.9.cloned.1.call-start = ((), (), s32[]{:S(2)}) async-start(), calls=%async_computation.4 | async-start | bytes 1179648 | tf_op jit(solution)/shard_map/all_gather | solution.py:65
  224.8 122.6 %all-gather.7.cloned.1.call-start = ((), (), s32[]{:S(2)}) async-start(), calls=%async_computation.3 | async-start | bytes 1179648 | tf_op jit(solution)/shard_map/all_gather | solution.py:64
  306.8 42.9 %copy-start.4 = (bf16[2048,256]{1,0:T(8,128)(2,1)S(1)}, bf16[2048,256]{1,0:T(8,128)(2,1)}, u32[]{:S(2)}) copy-start(bf16[2048,256]{1,0:T(8,128)(2,1)} %all-gather.9.cloned.1.call-done) | copy-start | bytes 3145732
Sparse Core Ops, SparseCore 0:
  10.2 62.7 all-gather.4
  89.1 62.6 reduce-scatter.1
  223.9 41.2 all-gather.10
  267.8 38.9 all-gather.8
  309.3 38.0 all-gather.6
where the time goes:
time: 358 us; the launch traced here: 357 us
  waiting for transfers between devices  246 us (69%)
  blocking collectives  68.8 us (19%)
  matrix products  16.7 us (5%)
  between operations  14.7 us (4%)
  local copies, waits for them, and re-layouts  8.36 us (2%)
    all_gather x1, waiting for transfers between devices, per_device(): whole_factors = lax.all_gather(factors, 'fs', axis=1, tiled=True)  65 us
    reduce_scatter x1, waiting for transfers between devices, per_device(): lax.psum_scatter(partial_sums, 'fs', scatter_dimension=1, tiled=True)  62.6 us
    all_gather x1, waiting for transfers between devices, per_device(): lax.all_gather(new_query, 'fs', axis=0, tiled=True)  40.6 us
    all_gather x1, waiting for transfers between devices, per_device(): lax.all_gather(new_key, 'fs', axis=0, tiled=True)  39.3 us
    all_gather x1, waiting for transfers between devices, per_device(): lax.all_gather(new_out, 'fs', axis=1, tiled=True)  37.6 us
    psum x1, blocking collectives, per_device(): square_total = lax.psum(jnp.sum(adam_ratio * adam_ratio), ('fs', 'tp'))  37.6 us
    all_gather x1, blocking collectives, per_device(): lax.all_gather(adam_ratio.astype(jnp.bfloat16), 'fs', axis=1, tiled=True)  31.2 us
    dot_general x3, matrix products, per_device(): jnp.dot(left_side, whole_factors[matrix_number], preferred_element_type=j...  11.1 us
  transfers between devices with their start and end apart: 5, of which 5 were waited for; matrix products, arithmetic and copies ran while one was open for 2% of the time, Pallas kernels for 0%

commit v1 on v0

--- a/solution.py
+++ b/solution.py
@@ -52,7 +52,7 @@
     reduced = lax.psum_scatter(partial_sums, "fs", scatter_dimension=1, tiled=True)
     first_new, second_new, adam_ratio = moments_update(reduced, moment_first, moment_second)
     square_total = lax.psum(jnp.sum(adam_ratio * adam_ratio), ("fs", "tp"))
-    directions = lax.all_gather(adam_ratio.astype(jnp.bfloat16), "fs", axis=1, tiled=True)
+    directions = jnp.concatenate(lax.all_gather(adam_ratio.astype(jnp.bfloat16), "fs"), axis=1)
     step_scale = lax.rsqrt(square_total / (3 * RANK * HW) + 1.0)
     step_query = step_scale * jnp.dot(factors[0], directions[0], preferred_element_type=jnp.float32)
     step_key = step_scale * jnp.dot(factors[1], directions[1], preferred_element_type=jnp.float32)

time: 358 us -> 358 us (level)
  no operation moved by 1% of the time
where the time goes in v1:
time: 358 us; the launch traced here: 357 us
  waiting for transfers between devices  246 us (69%)
  blocking collectives  68.8 us (19%)
  matrix products  16.7 us (5%)
  between operations  14.7 us (4%)
  local copies, waits for them, and re-layouts  8.39 us (2%)
    all_gather x1, waiting for transfers between devices, per_device(): whole_factors = lax.all_gather(factors, 'fs', axis=1, tiled=True)  65 us
    reduce_scatter x1, waiting for transfers between devices, per_device(): lax.psum_scatter(partial_sums, 'fs', scatter_dimension=1, tiled=True)  62.6 us
    all_gather x1, waiting for transfers between devices, per_device(): lax.all_gather(new_query, 'fs', axis=0, tiled=True)  40.6 us
    all_gather x1, waiting for transfers between devices, per_device(): lax.all_gather(new_key, 'fs', axis=0, tiled=True)  39.3 us
    psum x1, blocking collectives, per_device(): square_total = lax.psum(jnp.sum(adam_ratio * adam_ratio), ('fs', 'tp'))  37.7 us
    all_gather x1, waiting for transfers between devices, per_device(): lax.all_gather(new_out, 'fs', axis=1, tiled=True)  37.6 us
    all_gather x1, blocking collectives, per_device(): lax.all_gather(adam_ratio.astype(jnp.bfloat16), 'fs')  31.2 us
    dot_general x3, matrix products, per_device(): jnp.dot(left_side, whole_factors[matrix_number], preferred_element_type=j...  11.1 us
  transfers between devices with their start and end apart: 5, of which 5 were waited for; matrix products, arithmetic and copies ran while one was open for 2% of the time, Pallas kernels for 0%

profile of v1, /device:TPU:0, one launch (start us, length us, event | category | flops | bytes accessed | tf_op | source)
XLA Modules:
  0.0 357.3 jit_solution(6425890490261995462)
XLA Ops:
  7.2 0.0 copy-start
  7.2 0.0 all-gather.6.cloned.1.call-start
  7.2 0.7 all-gather.6.cloned.1.call-update
  7.9 0.0 reduce-scatter.2.cloned.1.call-start
  8.0 65.0 %all-gather.6.cloned.1.call-done = bf16[3,2048,256]{2,1,0:T(8,128)(2,1)} async-done(((bf16[3,256,256]{2,1,0:T(8,128)(2,1)}), bf16[3,2048,256]{2,1,0:T(8,128)(2,1)}) %all-gather.6.cloned.1.call-update) | async-done | bytes 3145744 | tf_op jit(solution)/shard_map/all_gather | solution.py:40
  73.0 0.0 copy-start.12
  73.0 6.2 %fusion.6 = f32[2048,256]{1,0:T(8,128)S(1)} fusion(bf16[2048,2048]{1,0:T(8,128)(2,1)} %param.11, bf16[3,2048,256]{2,1,0:T(8,128)(2,1)} %all-gather.6.cloned.1.call-done), kind=kOutput, calls=%fused_computation.17 | convolution fusion | flops 2147483648 | bytes 11534336 | tf_op jit(solution)/shard_map/dot_general | solution.py:43
  79.2 0.0 copy-done
  79.2 0.0 copy-start.13
  79.2 0.5 fusion.12
  79.7 0.0 slice-start
  79.7 0.5 fusion.3
  80.2 0.0 copy-done.12
  80.2 0.9 copy-done.13
  81.1 2.4 fusion.7
  83.6 0.0 copy-done.1
  83.6 0.5 fusion.15
  84.0 0.5 fusion.4
  84.5 0.0 slice-done
  84.5 0.0 slice-done.1
  84.6 0.0 copy-start.2
  84.6 2.4 fusion.5
  87.0 0.0 copy-done.2
  87.0 0.5 fusion.9
  87.5 0.5 fusion.2
  88.0 0.0 copy-start.8
  88.0 0.0 copy-start.10
  88.0 0.0 copy-start.11
  88.0 0.0 copy-start.3
  88.1 0.9 pad_maximum_fusion
  89.0 0.0 reduce-scatter.2.cloned.1.call-update
  89.0 0.0 all-gather.12.cloned.1.call-start
  89.1 0.0 copy-done.8
  89.1 0.1 copy.34
  89.2 0.0 copy-start.9
  89.2 62.6 %reduce-scatter.2.cloned.1.call-done = f32[3,32,256]{2,1,0:T(8,128)} async-done(((f32[3,256,256]{2,1,0:T(8,128)}), f32[3,32,256]{2,1,0:T(8,128)}) %reduce-scatter.2.cloned.1.call-update) | async-done | bytes 98320 | tf_op jit(solution)/shard_map/reduce_scatter | solution.py:52
  151.8 0.0 copy-done.10
  151.8 0.0 copy-done.11
  151.8 1.6 multiply_reduce_fusion
  153.4 31.2 %all-gather = bf16[24,32,256]{2,1,0:T(8,128)(2,1)S(1)} all-gather(bf16[3,32,256]{2,1,0:T(8,128)(2,1)S(1)} %fusion.24), channel_id=2, replica_groups=mesh['fs'=8,'tp'=4] {'fs'}, dimensions={0}, use_global_device_ids=true | all-gather | bytes 442368 | tf_op jit(solution)/shard_map/all_gather | solution.py:55
  184.7 37.7 %psum.7 = f32[]{:T(128)} all-reduce(f32[]{:T(128)} %get-tuple-element.24), channel_id=1, replica_groups=mesh['fs'=8,'tp'=4] {'fs','tp'}, use_global_device_ids=true, to_apply=%region_2.0 | all-reduce | flops 1 | bytes 8 | tf_op jit(solution)/shard_map/psum | solution.py:54
  223.0 0.0 copy-done.3
  223.0 0.9 subtract_convert_fusion.6
  223.9 0.0 all-gather.12.cloned.1.call-update
  223.9 0.0 all-gather.10.cloned.1.call-start
  223.9 0.0 copy-done.7
  223.9 0.9 subtract_convert_fusion.7
  224.9 0.0 all-gather.10.cloned.1.call-update
  224.9 0.0 all-gather.8.cloned.1.call-start
  225.0 0.0 copy-done.9
  225.0 0.1 copy.32
  225.1 0.9 subtract_convert_fusion.8
  226.0 0.0 copy-done.5
  226.0 0.0 copy-done.6
  226.0 0.0 all-gather.8.cloned.1.call-update
  226.0 0.8 copy.36
  226.9 0.8 copy.35
  227.7 37.6 %all-gather.12.cloned.1.call-done = bf16[256,2048]{0,1:T(8,128)(2,1)} async-done(((bf16[256,256]{0,1:T(8,128)(2,1)}), bf16[256,2048]{0,1:T(8,128)(2,1)}) %all-gather.12.cloned.1.call-update) | async-done | bytes 1048592 | tf_op jit(solution)/shard_map/all_gather | solution.py:66
  265.3 2.3 copy.38
  267.6 39.3 %all-gather.10.cloned.1.call-done = bf16[2048,256]{1,0:T(8,128)(2,1)} async-done(((bf16[256,256]{1,0:T(8,128)(2,1)}), bf16[2048,256]{1,0:T(8,128)(2,1)}) %all-gather.10.cloned.1.call-update) | async-done | bytes 1048592 | tf_op jit(solution)/shard_map/all_gather | solution.py:65
  306.9 40.6 %all-gather.8.cloned.1.call-done = bf16[2048,256]{0,1:T(8,128)(2,1)} async-done(((bf16[256,256]{0,1:T(8,128)(2,1)}), bf16[2048,256]{0,1:T(8,128)(2,1)}) %all-gather.8.cloned.1.call-update) | async-done | bytes 1048592 | tf_op jit(solution)/shard_map/all_gather | solution.py:64
  347.5 2.3 copy.37
  349.8 0.0 copy-done.4
  349.8 1.0 copy.42
  (9 shorter events, 0.1 us)
Async XLA Ops:
  7.2 72.0 %copy-start = (bf16[2048,256]{1,0:T(8,128)(2,1)S(1)}, bf16[2048,256]{1,0:T(8,128)(2,1)}, u32[]{:S(2)}) copy-start(bf16[2048,256]{1,0:T(8,128)(2,1)} %param.14) | copy-start | bytes 3145732
  7.2 65.8 %all-gather.6.cloned.1.call-start = ((), (), s32[]{:S(2)}) async-start(), calls=%async_computation.1 | async-start | bytes 3538944 | tf_op jit(solution)/shard_map/all_gather | solution.py:40
  7.9 143.9 %reduce-scatter.2.cloned.1.call-start = ((), (), s32[]{:S(2)}) async-start(), calls=%async_computation.2 | async-start | bytes 884736 | tf_op jit(solution)/shard_map/reduce_scatter | solution.py:52
  73.0 7.3 %copy-start.12 = (bf16[2048,2048]{1,0:T(8,128)(2,1)S(1)}, bf16[2048,2048]{1,0:T(8,128)(2,1)}, u32[]{:S(2)}) copy-start(bf16[2048,2048]{1,0:T(8,128)(2,1)} %param.11) | copy-start | bytes 25165828
  79.2 1.9 copy-start.13
  79.7 4.8 %slice-start = ((s8[8388608]{0:T(1024)(128)(4,1)}), s8[4194304]{0:T(1024)(128)(4,1)S(1)}, s32[]{:S(2)}) async-start(s8[8388608]{0:T(1024)(128)(4,1)} %bitcast.56), calls=%async_computation.6 | async-start | bytes 8388608
  81.1 2.5 copy-start.1
  81.1 3.4 slice-start.1
  84.6 2.5 copy-start.2
  88.0 1.1 copy-start.8
  88.0 63.8 %copy-start.10 = (f32[3,32,256]{2,1,0:T(8,128)S(1)}, f32[3,32,256]{2,1,0:T(8,128)}, u32[]{:S(2)}) copy-start(f32[3,32,256]{2,1,0:T(8,128)} %param.21) | copy-start | bytes 294916
  88.0 63.8 %copy-start.11 = (f32[3,32,256]{2,1,0:T(8,128)S(1)}, f32[3,32,256]{2,1,0:T(8,128)}, u32[]{:S(2)}) copy-start(f32[3,32,256]{2,1,0:T(8,128)} %param.20) | copy-start | bytes 294916
  88.0 135.0 %copy-start.3 = (bf16[3,256,256]{2,1,0:T(8,128)(2,1)S(1)}, bf16[3,256,256]{2,1,0:T(8,128)(2,1)}, u32[]{:S(2)}) copy-start(bf16[3,256,256]{2,1,0:T(8,128)(2,1)} %param.19) | copy-start | bytes 1179652
  89.0 135.0 %copy-start.7 = (f32[256,256]{1,0:T(8,128)S(1)}, f32[256,256]{1,0:T(8,128)}, u32[]{:S(2)}) copy-start(f32[256,256]{1,0:T(8,128)} %param.17) | copy-start | bytes 786436
  89.0 176.3 %all-gather.12.cloned.1.call-start = ((), (), s32[]{:S(2)}) async-start(), calls=%async_computation.5 | async-start | bytes 1179648 | tf_op jit(solution)/shard_map/all_gather | solution.py:66
  89.2 135.8 %copy-start.9 = (f32[256,256]{1,0:T(8,128)S(1)}, f32[256,256]{1,0:T(8,128)}, u32[]{:S(2)}) copy-start(f32[256,256]{1,0:T(8,128)} %param.16) | copy-start | bytes 786436
  153.4 72.6 %copy-start.5 = (f32[3,32,256]{2,1,0:T(8,128)}, f32[3,32,256]{2,1,0:T(8,128)S(1)}, u32[]{:S(2)}) copy-start(f32[3,32,256]{2,1,0:T(8,128)S(1)} %get-tuple-element.51) | copy-start | bytes 294916
  153.4 72.6 %copy-start.6 = (f32[3,32,256]{2,1,0:T(8,128)}, f32[3,32,256]{2,1,0:T(8,128)S(1)}, u32[]{:S(2)}) copy-start(f32[3,32,256]{2,1,0:T(8,128)S(1)} %get-tuple-element.50) | copy-start | bytes 294916
  223.9 83.0 %all-gather.10.cloned.1.call-start = ((), (), s32[]{:S(2)}) async-start(), calls=%async_computation.4 | async-start | bytes 1179648 | tf_op jit(solution)/shard_map/all_gather | solution.py:65
  224.9 122.6 %all-gather.8.cloned.1.call-start = ((), (), s32[]{:S(2)}) async-start(), calls=%async_computation.3 | async-start | bytes 1179648 | tf_op jit(solution)/shard_map/all_gather | solution.py:64
  306.9 42.9 %copy-start.4 = (bf16[2048,256]{1,0:T(8,128)(2,1)S(1)}, bf16[2048,256]{1,0:T(8,128)(2,1)}, u32[]{:S(2)}) copy-start(bf16[2048,256]{1,0:T(8,128)(2,1)} %all-gather.10.cloned.1.call-done) | copy-start | bytes 3145732
Sparse Core Ops, SparseCore 0:
  10.2 62.7 all-gather.5
  89.1 62.6 reduce-scatter.1
  224.0 41.2 all-gather.11
  267.9 38.9 all-gather.9
  309.4 38.0 all-gather.7
